TPU v7x, 512 devices: a whole 4x8x8 slice. The times are simulated.
512 devices in a mesh: sp: 32 (over z, x), tp: 16 (over y, core).
Axes of the slice: x: 4, y: 8, z: 8, core: 2. Of those that a mesh axis runs over, the one named last changes fastest.
Arguments:
- target_rows: bfloat16 [2048, 2048], P(('sp', 'tp')), may hold values from -6 to 6
- source_rows: bfloat16 [8192, 2048], P(('sp', 'tp')), may hold values from -6 to 6
- norm_gain: bfloat16 [2048], replicated, may hold values from 0.099609375 to 1.8984375
- query_weight: bfloat16 [2048, 4096], P(None, 'tp'), may hold values from -0.125 to 0.125
- key_weight: bfloat16 [2048, 4096], P(None, 'tp'), may hold values from -0.125 to 0.125
- value_weight: bfloat16 [2048, 4096], P(None, 'tp'), may hold values from -0.125 to 0.125
- output_weight: bfloat16 [4096, 2048], P('tp'), may hold values from -0.09375 to 0.09375
- saved_output: bfloat16 [2048, 4096], P('sp', 'tp'), may hold values from -3 to 3
- norm_offset: bfloat16 [2048, 16], P('sp', 'tp'), may hold values from 0.25 to 1.25
- output_grad: bfloat16 [2048, 2048], P(('sp', 'tp')), may hold values from -192 to 192
Outputs:
- target_grad: float32 [2048, 2048], P(('sp', 'tp'))
- source_grad: float32 [8192, 2048], P(('sp', 'tp'))
- query_weight_grad: float32 [2048, 4096], P('sp', 'tp')
All inputs are finite; a program needn't handle non-finite values.
Results may differ from a plain program's by a relative error of at most 0.033.
Values may be sent and summed in bfloat16 or wider, within the bound.
A program may use at most 64 MiB of HBM per device.

v0:
```python
import math
import jax
import jax.numpy as jnp
from jax import lax
from jax.sharding import Mesh
from jax.sharding import PartitionSpec as P

HEAD_DIM = 256
SP = ("sp_0", "sp_1")
SP_TP = ("sp_0", "sp_1", "tp")
EPSILON = 1e-06


def from_everyone(shard, axis):
    copies = jnp.broadcast_to(shard, (lax.axis_size(axis), *shard.shape))
    return lax.all_to_all(copies, axis, split_axis=0, concat_axis=0, tiled=True)


def in_order(parts, dim):
    parts = jnp.moveaxis(parts, 0, dim)
    dims = parts.shape
    return parts.reshape(*dims[:dim], dims[dim] * dims[dim + 1], *dims[dim + 2 :])


def gathered_copies(shard, axis, dim):
    parts = from_everyone(shard, axis)
    return in_order(parts, dim)


def side_by_side(arrays, axis, dim, along):
    widths = [math.prod(a.shape[along:]) for a in arrays]
    both = jnp.concatenate(
        [a.reshape(*a.shape[:along], w) for a, w in zip(arrays, widths)], axis=along
    )
    whole = lax.all_gather(both, axis, axis=dim, tiled=True)
    parts = jnp.split(whole, [sum(widths[:k]) for k in range(1, len(widths))], axis=along)
    return tuple((b.reshape(*whole.shape[:along], *a.shape[along:]) for a, b in zip(arrays, parts)))


def sum_by_axis(shard, axes, dim):
    if not axes:
        return shard
    nearer = lax.psum_scatter(shard, axes[0], scatter_dimension=dim, tiled=True)
    return sum_by_axis(nearer, axes[1:], dim)


def cut_along(shard, dim, size):
    before, after = (shard.shape[:dim], shard.shape[dim + 1 :])
    return jnp.moveaxis(shard.reshape(*before, size, -1, *after), dim, 0)


def sum_at_owner(shard, axis, dim):
    size = lax.axis_size(axis)
    parts = lax.all_to_all(cut_along(shard, dim, size), axis, 0, 0, tiled=True)
    return jnp.sum(parts.astype(jnp.float32), axis=0)


def sum_at_owner_2(shard, axis, dim):
    size = lax.axis_size(axis)
    parts = lax.all_to_all(cut_along(shard, dim, size), axis, 0, 0, tiled=True)
    return jnp.sum(parts, axis=0)


def contract_last(left, right):
    return lax.dot_general(
        left, right, (((1,), (1,)), ((), ())), preferred_element_type=jnp.float32
    )


def attention_weights(
    query_rows, head_gradient, offsets, deltas, key_row_block, value_row_block, shift_base
):
    score_scale = HEAD_DIM ** (-0.5)
    score_matrix = jnp.einsum(
        "rfo,kfo->frk", query_rows, key_row_block, preferred_element_type=jnp.float32
    )
    shifts = jnp.transpose(shift_base + offsets.astype(jnp.float32))[:, :, None]
    prob_rows = jnp.exp(score_matrix * score_scale - shifts)
    prob_grad = jnp.einsum(
        "rfo,kfo->frk", head_gradient, value_row_block, preferred_element_type=jnp.float32
    )
    score_grad = (
        prob_rows
        * (prob_grad - jnp.transpose(deltas.astype(jnp.float32))[:, :, None])
        * score_scale
    )
    return (prob_rows.astype(jnp.bfloat16), score_grad.astype(jnp.bfloat16))


def body(
    target_rows,
    source_rows,
    norm_gain,
    query_weight,
    key_weight,
    value_weight,
    output_weight,
    saved_output,
    norm_offset,
    output_grad,
):
    tp_count = lax.axis_size("tp")
    sp_count = lax.axis_size(SP)
    query_width = query_weight.shape[1]
    local_heads = query_width // HEAD_DIM
    target_count = saved_output.shape[0]
    source_count = source_rows.shape[0] * tp_count
    shift_base = math.log(source_count * sp_count)
    target_float = target_rows.astype(jnp.float32)
    gain_float = norm_gain.astype(jnp.float32)
    inverse = lax.rsqrt(jnp.mean(target_float * target_float, axis=1, keepdims=True) + EPSILON)
    normed = (target_float * inverse * gain_float).astype(jnp.bfloat16)
    slice_share = lax.all_gather(jnp.stack([normed, output_grad]), "tp", axis=1, tiled=True)
    query_part = jnp.dot(slice_share[0], query_weight, preferred_element_type=jnp.float32).astype(
        jnp.bfloat16
    )
    grad_part = contract_last(slice_share[1], output_weight).astype(jnp.bfloat16)
    joined = jnp.concatenate([query_part, grad_part, slice_share[0]], axis=1)
    query_rows = joined[:, :query_width].reshape(target_count, local_heads, HEAD_DIM)
    head_gradient = joined[:, query_width : 2 * query_width].reshape(
        target_count, local_heads, HEAD_DIM
    )
    normed_all = joined[:, 2 * query_width :]
    saved_heads = saved_output.reshape(target_count, local_heads, HEAD_DIM)
    deltas = jnp.sum(
        head_gradient.astype(jnp.float32) * saved_heads.astype(jnp.float32), axis=2
    ).astype(jnp.bfloat16)
    slice_share = gathered_copies(source_rows, "tp", 0)
    key_part = jnp.dot(slice_share, key_weight, preferred_element_type=jnp.float32).astype(
        jnp.bfloat16
    )
    value_part = jnp.dot(slice_share, value_weight, preferred_element_type=jnp.float32).astype(
        jnp.bfloat16
    )
    projected = jnp.concatenate([key_part, value_part], axis=1)
    key_row_block = projected[:, :query_width].reshape(source_count, local_heads, HEAD_DIM)
    value_row_block = projected[:, query_width:].reshape(source_count, local_heads, HEAD_DIM)
    slice_share = side_by_side((query_rows, head_gradient, norm_offset, deltas), SP, 0, 2)
    probability_rounded, score_rounded = attention_weights(
        slice_share[0],
        slice_share[1],
        slice_share[2],
        slice_share[3],
        key_row_block,
        value_row_block,
        shift_base,
    )
    key_total = jnp.einsum(
        "wcu,cwp->uwp", score_rounded, slice_share[0], preferred_element_type=jnp.float32
    )
    value_total = jnp.einsum(
        "wcu,cwp->uwp", probability_rounded, slice_share[1], preferred_element_type=jnp.float32
    )
    key_total, value_total, score_rounded = (key_total, value_total, score_rounded)
    query_term = jnp.einsum(
        "tje,etq->jtq", score_rounded, key_row_block, preferred_element_type=jnp.float32
    )
    query_grad = sum_by_axis(query_term.astype(jnp.bfloat16), SP, 0).astype(jnp.float32)
    query_flat = query_grad.astype(jnp.bfloat16).reshape(target_count, query_width)
    normed_grad = sum_at_owner(
        contract_last(query_flat, query_weight).astype(jnp.bfloat16), "tp", 0
    )
    scaled = normed_grad * gain_float
    target_grad = inverse * scaled - target_float * inverse**3 * jnp.mean(
        scaled * target_float, axis=1, keepdims=True
    )
    key_flat = key_total.astype(jnp.bfloat16).reshape(source_count, query_width)
    value_flat = value_total.astype(jnp.bfloat16).reshape(source_count, query_width)
    key_part = contract_last(key_flat, key_weight)
    value_part = contract_last(value_flat, value_weight)
    source_grad = sum_at_owner((key_part + value_part).astype(jnp.bfloat16), "tp", 0)
    weight_grad = sum_at_owner_2(
        lax.dot_general(
            normed_all, query_flat, (((0,), (0,)), ((), ())), preferred_element_type=jnp.float32
        ),
        SP,
        0,
    )
    return (target_grad, source_grad, weight_grad)


def solution(mesh):
    split = Mesh(mesh.devices.reshape(8, 4, mesh.shape["tp"]), ("sp_0", "sp_1", "tp"))
    placed = (
        P(SP_TP, None),
        P(SP_TP, None),
        P(),
        P(None, "tp"),
        P(None, "tp"),
        P(None, "tp"),
        P("tp", None),
        P(SP, "tp"),
        P(SP, "tp"),
        P(SP_TP, None),
    )
    return jax.shard_map(
        body,
        mesh=split,
        in_specs=placed,
        out_specs=(P(SP_TP, None), P(SP_TP, None), P(SP, "tp")),
        check_vma=False,
    )
```

profile of v0, /device:TPU:3, one launch (start us, length us, event | category | flops | bytes accessed | tf_op | source)
XLA Modules:
  0.0 286.7 jit_solution(7998154061447127349)
XLA Ops:
  7.2 0.0 copy-start
  7.2 0.0 all-gather.2.cloned.1.call-start
  7.2 1.0 fusion.13
  8.2 0.7 convert_element_type.117
  8.9 0.8 fusion.21
  9.7 0.0 copy-start.3
  9.7 0.8 pad_maximum_fusion.1
  10.6 0.8 copy.28
  11.4 19.5 %all_gather.6 = bf16[2,64,2048]{2,0,1:T(2,128)(2,1)S(1)} all-gather(bf16[2,4,2048]{2,0,1:T(2,128)(2,1)S(1)} %copy.25), channel_id=1, replica_groups=mesh['sp_0'=8,'sp_1'=4,'tp'=16] {'tp'}, dimensions={1}, use_global_device_ids=true | all-gather | bytes 557056 | tf_op jit(solution)/shard_map/all_gather | solution.py:113
  30.9 1.6 fusion.22
  32.5 0.6 multiply_reduce_fusion
  33.1 0.1 copy.29
  33.2 0.0 copy-start.1
  33.2 1.5 fusion.10
  34.7 0.7 pad_maximum_fusion
  35.4 0.0 all-gather.2.cloned.1.call-update
  35.4 0.0 reduce-scatter.5.cloned.1.call-start
  35.5 0.1 broadcast_in_dim.2
  35.6 32.7 %all_to_all.20 = bf16[16,16,2048]{2,1,0:T(8,128)(2,1)S(1)} all-to-all(bf16[16,16,2048]{2,1,0:T(8,128)(2,1)S(1)} %broadcast_in_dim.2), channel_id=1, replica_groups=mesh['sp_0'=8,'sp_1'=4,'tp'=16] {'tp'}, dimensions={0} | all-to-all | bytes 2097152 | tf_op jit(solution)/shard_map/all_to_all | solution.py:16
  68.3 0.4 convolution_convert_fusion.5
  68.8 47.4 %all-gather.2.cloned.1.call-done = bf16[2048,1,514]{2,0,1:T(8,128)(2,1)} async-done(((bf16[64,1,514]{2,0,1:T(8,128)(2,1)}), bf16[2048,1,514]{2,0,1:T(8,128)(2,1)}) %all-gather.2.cloned.1.call-update) | async-done | bytes 2105360 | tf_op jit(solution)/shard_map/all_gather | solution.py:35
  116.2 1.9 convert_reduce_fusion.1
  118.0 3.1 %fusion.3 = f32[2048,256]{1,0:T(8,128)} fusion(bf16[256,256]{1,0:T(8,128)(2,1)S(1)} %convolution_convert_fusion.5, f32[2048]{0:T(1024)S(1)} %get-tuple-element.4, bf16[2048,1,514]{2,0,1:T(8,128)(2,1)} %all-gather.2.cloned.1.call-done), kind=kOutput, calls=%fused_computation.6 | convolution fusion | flops 269484032 | bytes 3284992 | tf_op jit(solution)/shard_map/rfo,kfo->frk/dot_general | solution.py:74
  121.1 3.3 %fusion.5 = bf16[2048,256]{1,0:T(8,128)(2,1)S(1)} fusion(f32[2048,256]{1,0:T(8,128)} %fusion.3, bf16[256,2048]{1,0:T(8,128)(2,1)S(1)} %bitcast.80, bf16[2048,256]{1,0:T(8,128)(2,1)S(1)} %copy-done, f32[2048]{0:T(1024)S(1)} %get-tuple-element.3, bf16[2048,1,514]{2,0,1:T(8,128)(2,1)} %all-gather.2.cloned.1.call-done), kind=kOutput, calls=%fused_computation.9 | convolution fusion | flops 539033600 | bytes 6299648 | tf_op jit(solution)/shard_map/rfo,kfo->frk/dot_general | solution.py:79
  124.4 0.0 copy-start.2
  124.4 1.6 fusion.6
  126.0 0.0 reduce-scatter.5.cloned.1.call-update
  126.0 4.0 %fusion.8 = f32[256,2048]{1,0:T(8,128)} fusion(bf16[2048,256]{1,0:T(8,128)(2,1)S(1)} %copy-done.2, bf16[2048,256]{1,0:T(8,128)(2,1)S(1)} %fusion.5, bf16[2048,1,514]{2,0,1:T(8,128)(2,1)} %all-gather.2.cloned.1.call-done), kind=kOutput, calls=%fused_computation.18 | convolution fusion | flops 536936448 | bytes 5242880 | tf_op jit(solution)/shard_map/dot_general | solution.py:65
  130.0 4.9 %fusion.4 = bf16[256,2048]{1,0:T(8,128)(2,1)} fusion(f32[256,2048]{1,0:T(8,128)} %fusion.8, bf16[2048,256]{1,0:T(8,128)(2,1)S(1)} %copy-done, f32[2048,256]{1,0:T(8,128)} %fusion.3, bf16[2048,1,514]{2,0,1:T(8,128)(2,1)} %all-gather.2.cloned.1.call-done), kind=kOutput, calls=%fused_computation.7 | convolution fusion | flops 538509312 | bytes 7340032 | tf_op jit(solution)/shard_map/dot_general | solution.py:65
  134.9 11.8 %all-to-all-start.2 = ((bf16[16,16,2048]{2,1,0:T(8,128)(2,1)}), bf16[16,16,2048]{2,1,0:T(8,128)(2,1)S(1)}, u32[]{:S(2)}, u32[]{:S(2)}) async-start(bf16[16,16,2048]{2,1,0:T(8,128)(2,1)} %bitcast.20), calls=%async_computation.3 | async-start | bytes 2097152 | tf_op jit(solution)/shard_map/all_to_all | solution.py:54
  146.7 0.0 reduce-scatter.7.cloned.1.call-start
  146.7 19.3 %reduce-scatter.5.cloned.1.call-done = bf16[256,1,256]{0,2,1:T(8,128)(2,1)} async-done(((bf16[2048,1,256]{0,2,1:T(8,128)(2,1)}), bf16[256,1,256]{0,2,1:T(8,128)(2,1)}) %reduce-scatter.5.cloned.1.call-update) | async-done | bytes 131088 | tf_op jit(solution)/shard_map/reduce_scatter | solution.py:43
  166.0 1.7 copy.36
  167.7 0.0 reduce-scatter.7.cloned.1.call-update
  167.7 26.5 %reduce-scatter.7.cloned.1.call-done = bf16[64,256]{1,0:T(8,128)(2,1)} async-done(((bf16[256,256]{1,0:T(8,128)(2,1)}), bf16[64,256]{1,0:T(8,128)(2,1)}) %reduce-scatter.7.cloned.1.call-update) | async-done | bytes 32784 | tf_op jit(solution)/shard_map/reshape | solution.py:159
  194.2 1.3 convolution_convert_fusion.1
  195.5 0.8 reshape.145
  196.3 9.5 %all-to-all-start.1 = ((bf16[16,4,2048]{2,1,0:T(4,128)(2,1)}), bf16[16,4,2048]{2,1,0:T(4,128)(2,1)S(1)}, u32[]{:S(2)}, u32[]{:S(2)}) async-start(bf16[16,4,2048]{2,1,0:T(4,128)(2,1)} %reshape.145), calls=%async_computation.2 | async-start | bytes 524288 | tf_op jit(solution)/shard_map/all_to_all | solution.py:54
  205.8 1.4 copy.40
  207.2 1.8 fusion.19
  209.0 8.4 %all-to-all-done.1 = bf16[16,4,2048]{2,1,0:T(4,128)(2,1)S(1)} async-done(((bf16[16,4,2048]{2,1,0:T(4,128)(2,1)}), bf16[16,4,2048]{2,1,0:T(4,128)(2,1)S(1)}, u32[]{:S(2)}, u32[]{:S(2)}) %all-to-all-start.1) | async-done | bytes 262176 | tf_op jit(solution)/shard_map/all_to_all | solution.py:54
  217.4 10.3 %all-to-all-start.3 = ((f32[32,64,256]{2,1,0:T(8,128)}), f32[32,64,256]{2,1,0:T(8,128)S(1)}, u32[]{:S(2)}, u32[]{:S(2)}) async-start(f32[32,64,256]{2,1,0:T(8,128)} %fusion.19), calls=%async_computation.4 | async-start | bytes 4194304 | tf_op jit(solution)/shard_map/all_to_all | solution.py:60
  227.6 2.0 convert_reduce_fusion
  229.7 0.1 convert_reduce_fusion.2
  229.8 0.1 fusion.18
  229.9 0.7 fusion.17
  230.6 48.7 %all-to-all-done.3 = f32[32,64,256]{2,1,0:T(8,128)S(1)} async-done(((f32[32,64,256]{2,1,0:T(8,128)}), f32[32,64,256]{2,1,0:T(8,128)S(1)}, u32[]{:S(2)}, u32[]{:S(2)}) %all-to-all-start.3) | async-done | bytes 2097184 | tf_op jit(solution)/shard_map/all_to_all | solution.py:60
  279.4 0.8 reduce_sum.59
  (22 shorter events, 0.1 us)
Async XLA Ops:
  7.2 114.0 %copy-start = (bf16[2048,256]{1,0:T(8,128)(2,1)S(1)}, bf16[2048,256]{1,0:T(8,128)(2,1)}, u32[]{:S(2)}) copy-start(bf16[2048,256]{1,0:T(8,128)(2,1)} %param.15) | copy-start | bytes 3145732
  7.2 25.3 %copy-start.10 = (bf16[64,256]{1,0:T(8,128)(2,1)S(1)}, bf16[64,256]{1,0:T(8,128)(2,1)}, u32[]{:S(2)}) copy-start(bf16[64,256]{1,0:T(8,128)(2,1)} %param.17) | copy-start | bytes 98308
  7.2 25.3 %copy-start.6 = (bf16[256,2048]{1,0:T(8,128)(2,1)S(1)}, bf16[256,2048]{1,0:T(8,128)(2,1)}, u32[]{:S(2)}) copy-start(bf16[256,2048]{1,0:T(8,128)(2,1)} %param.16) | copy-start | bytes 3145732
  7.2 109.0 %all-gather.2.cloned.1.call-start = ((), (), s32[]{:S(2)}) async-start(), calls=%async_computation.6 | async-start | bytes 2703360 | tf_op jit(solution)/shard_map/all_gather | solution.py:35
  9.7 23.5 %copy-start.3 = (bf16[2048,256]{1,0:T(8,128)(2,1)S(1)}, bf16[2048,256]{1,0:T(8,128)(2,1)}, u32[]{:S(2)}) copy-start(bf16[2048,256]{1,0:T(8,128)(2,1)} %param.13) | copy-start | bytes 3145732
  30.9 4.6 %copy-start.9 = (bf16[16,2048]{1,0:T(8,128)(2,1)S(1)}, bf16[16,2048]{1,0:T(8,128)(2,1)}, u32[]{:S(2)}) copy-start(bf16[16,2048]{1,0:T(8,128)(2,1)} %param.11) | copy-start | bytes 196612
  33.2 35.1 %copy-start.1 = (bf16[2048,256]{1,0:T(8,128)(2,1)S(1)}, bf16[2048,256]{1,0:T(8,128)(2,1)}, u32[]{:S(2)}) copy-start(bf16[2048,256]{1,0:T(8,128)(2,1)} %param.14) | copy-start | bytes 3145732
  35.4 130.6 %reduce-scatter.5.cloned.1.call-start = ((), (), s32[]{:S(2)}) async-start(), calls=%async_computation.7 | async-start | bytes 1179648 | tf_op jit(solution)/shard_map/reduce_scatter | solution.py:43
  124.4 1.6 copy-start.2
  134.9 59.3 %copy-start.4 = (bf16[2048,256]{1,0:T(8,128)(2,1)S(1)}, bf16[2048,256]{1,0:T(8,128)(2,1)}, u32[]{:S(2)}) copy-start(bf16[2048,256]{1,0:T(8,128)(2,1)} %param.13) | copy-start | bytes 3145732
  134.9 61.3 %all-to-all-start.2 = ((bf16[16,16,2048]{2,1,0:T(8,128)(2,1)}), bf16[16,16,2048]{2,1,0:T(8,128)(2,1)S(1)}, u32[]{:S(2)}, u32[]{:S(2)}) async-start(bf16[16,16,2048]{2,1,0:T(8,128)(2,1)} %bitcast.20), calls=%async_computation.3 | async-start | bytes 2097152 | tf_op jit(solution)/shard_map/all_to_all | solution.py:54
  146.7 47.5 %reduce-scatter.7.cloned.1.call-start = ((), (), s32[]{:S(2)}) async-start(), calls=%async_computation.8 | async-start | bytes 163840 | tf_op jit(solution)/shard_map/reshape | solution.py:159
  194.2 13.0 %copy-start.8 = (bf16[64,256]{1,0:T(8,128)(2,1)S(1)}, bf16[64,256]{1,0:T(8,128)(2,1)}, u32[]{:S(2)}) copy-start(bf16[64,256]{1,0:T(8,128)(2,1)} %reduce-scatter.7.cloned.1.call-done) | copy-start | bytes 98308
  196.3 12.7 %copy-start.5 = (bf16[16,16,2048]{2,1,0:T(8,128)(2,1)}, bf16[16,16,2048]{2,1,0:T(8,128)(2,1)S(1)}, u32[]{:S(2)}) copy-start(bf16[16,16,2048]{2,1,0:T(8,128)(2,1)S(1)} %all-to-all-done.2) | copy-start | bytes 3145732
  196.3 21.1 %all-to-all-start.1 = ((bf16[16,4,2048]{2,1,0:T(4,128)(2,1)}), bf16[16,4,2048]{2,1,0:T(4,128)(2,1)S(1)}, u32[]{:S(2)}, u32[]{:S(2)}) async-start(bf16[16,4,2048]{2,1,0:T(4,128)(2,1)} %reshape.145), calls=%async_computation.2 | async-start | bytes 524288 | tf_op jit(solution)/shard_map/all_to_all | solution.py:54
  209.0 20.8 %copy-start.7 = (bf16[4,2048]{1,0:T(4,128)(2,1)S(1)}, bf16[4,2048]{1,0:T(4,128)(2,1)}, u32[]{:S(2)}) copy-start(bf16[4,2048]{1,0:T(4,128)(2,1)} %param.10) | copy-start | bytes 49156
  217.4 62.0 %all-to-all-start.3 = ((f32[32,64,256]{2,1,0:T(8,128)}), f32[32,64,256]{2,1,0:T(8,128)S(1)}, u32[]{:S(2)}, u32[]{:S(2)}) async-start(f32[32,64,256]{2,1,0:T(8,128)} %fusion.19), calls=%async_computation.4 | async-start | bytes 4194304 | tf_op jit(solution)/shard_map/all_to_all | solution.py:60
Sparse Core Ops, SparseCore 0:
  35.6 80.5 all-gather.1
  126.1 39.8 reduce-scatter.4
  169.4 24.7 reduce-scatter.6
where the time goes:
time: 287 us
  waiting for transfers between devices  150 us (52%)
  blocking collectives  52.2 us (18%)
  starting transfers between devices  31.6 us (11%)
  matrix products  22.3 us (8%)
  between operations  13.9 us (5%)
  other arithmetic  9.66 us (3%)
  local copies, waits for them, and re-layouts  6.56 us (2%)
    all_to_all x1, waiting for transfers between devices, sum_at_owner_2(): parts = lax.all_to_all(cut_along(shard, dim, size), axis, 0, 0, tiled=True)  48.7 us
    all_gather x1, waiting for transfers between devices, side_by_side(): whole = lax.all_gather(both, axis, axis=dim, tiled=True)  47.4 us
    all_to_all x1, blocking collectives, from_everyone(): return lax.all_to_all(copies, axis, split_axis=0, concat_axis=0, tiled=True)  32.7 us
    reshape x1, waiting for transfers between devices, body(): query_grad.astype(jnp.bfloat16).reshape(target_count, query_width)  26.5 us
    all_to_all x2, starting transfers between devices, sum_at_owner(): parts = lax.all_to_all(cut_along(shard, dim, size), axis, 0, 0, tiled=True)  21.3 us
    all_gather x1, blocking collectives, body(): lax.all_gather(jnp.stack([normed, output_grad]), 'tp', axis=1, tiled=True)  19.5 us
    reduce_scatter x1, waiting for transfers between devices, sum_by_axis(): nearer = lax.psum_scatter(shard, axes[0], scatter_dimension=dim, tiled=True)  19.3 us
    dot_general x4, matrix products, contract_last(): lax.dot_general(left, right, (((1,), (1,)), ((), ())), preferred_element_...  10.7 us
  transfers between devices with their start and end apart: 6, of which 5 were waited for; matrix products, arithmetic and copies ran while one was open for 7% of the time, Pallas kernels for 0%

commit v1 on v0

--- a/solution.py
+++ b/solution.py
@@ -110,7 +110,25 @@
     gain_float = norm_gain.astype(jnp.float32)
     inverse = lax.rsqrt(jnp.mean(target_float * target_float, axis=1, keepdims=True) + EPSILON)
     normed = (target_float * inverse * gain_float).astype(jnp.bfloat16)
-    slice_share = lax.all_gather(jnp.stack([normed, output_grad]), "tp", axis=1, tiled=True)
+    value = jnp.stack([normed, output_grad])
+    size_2, index, extent = (lax.axis_size("tp"), lax.axis_index("tp"), value.shape[1])
+    ahead = [(i, (i + 1) % size_2) for i in range(size_2)]
+    backward = [(i, (i - 1) % size_2) for i in range(size_2)]
+    result = jnp.zeros((*value.shape[:1], size_2 * extent, *value.shape[1 + 1 :]), value.dtype)
+    result = lax.dynamic_update_slice_in_dim(result, value, index * extent, axis=1)
+    from_left = from_right = value
+    halfway = size_2 // 2
+    for lap in range(1, halfway + 1):
+        from_left = lax.ppermute(from_left, "tp", ahead)
+        result = lax.dynamic_update_slice_in_dim(
+            result, from_left, (index - lap) % size_2 * extent, axis=1
+        )
+        if lap < size_2 - halfway:
+            from_right = lax.ppermute(from_right, "tp", backward)
+            result = lax.dynamic_update_slice_in_dim(
+                result, from_right, (index + lap) % size_2 * extent, axis=1
+            )
+    slice_share = result
     query_part = jnp.dot(slice_share[0], query_weight, preferred_element_type=jnp.float32).astype(
         jnp.bfloat16
     )

time: 287 us -> 434 us (1.51)
  local copies, waits for them, and re-layouts: 6.56 us -> 134 us
  starting transfers between devices: 31.6 us -> 53.6 us
  blocking collectives: 52.2 us -> 40.6 us
  waiting for transfers between devices: 150 us -> 157 us
    dynamic_update_slice x0 -> x16, local copies, waits for them, and re-layouts: none -> 119 us  [the longest x8 59.9 us: body(): lax.dynamic_update_slice_in_dim(result, from_left, (index - lap) % size_2...]
    ppermute x0 -> x15, starting transfers between devices: none -> 22 us  [the longest x7 13.9 us: body(): from_right = lax.ppermute(from_right, 'tp', backward)]
    all_gather x1 -> x0, blocking collectives: 19.5 us -> none  [body(): lax.all_gather(jnp.stack([normed, output_grad]), 'tp', axis=1, tiled=True)]
    ppermute x0 -> x15, local copies, waits for them, and re-layouts: none -> 10.1 us  [the longest x8 5.77 us: body(): from_left = lax.ppermute(from_left, 'tp', ahead)]
    all_to_all x1, blocking collectives: 32.7 us -> 40.6 us  [from_everyone(): return lax.all_to_all(copies, axis, split_axis=0, concat_axis=0, tiled=True)]
    ppermute x0 -> x15, waiting for transfers between devices: none -> 6.68 us  [the longest x8 5.44 us: body(): from_left = lax.ppermute(from_left, 'tp', ahead)]
  transfers between devices with their start and end apart: 6 -> 21, of which waited for: 5 -> 17; matrix products, arithmetic and copies ran while one was open for 7% -> 32% of each run, Pallas kernels for 0% -> 0%
where the time goes in v1:
time: 434 us; the launch traced here: 433 us
  waiting for transfers between devices  157 us (36%)
  local copies, waits for them, and re-layouts  134 us (31%)
  starting transfers between devices  53.6 us (12%)
  blocking collectives  40.6 us (9%)
  matrix products  24 us (6%)
  between operations  14.5 us (3%)
  other arithmetic  9.51 us (2%)
    dynamic_update_slice x8, local copies, waits for them, and re-layouts, body(): lax.dynamic_update_slice_in_dim(result, from_left, (index - lap) % size_2...  59.9 us
    dynamic_update_slice x7, local copies, waits for them, and re-layouts, body(): lax.dynamic_update_slice_in_dim(result, from_right, (index + lap) % size_...  52 us
    all_to_all x1, waiting for transfers between devices, sum_at_owner_2(): parts = lax.all_to_all(cut_along(shard, dim, size), axis, 0, 0, tiled=True)  48.7 us
    all_gather x1, waiting for transfers between devices, side_by_side(): whole = lax.all_gather(both, axis, axis=dim, tiled=True)  46.2 us
    all_to_all x1, blocking collectives, from_everyone(): return lax.all_to_all(copies, axis, split_axis=0, concat_axis=0, tiled=True)  40.6 us
    reshape x1, waiting for transfers between devices, body(): query_grad.astype(jnp.bfloat16).reshape(target_count, query_width)  26.3 us
    all_to_all x2, starting transfers between devices, sum_at_owner(): parts = lax.all_to_all(cut_along(shard, dim, size), axis, 0, 0, tiled=True)  21.2 us
    reduce_scatter x1, waiting for transfers between devices, sum_by_axis(): nearer = lax.psum_scatter(shard, axes[0], scatter_dimension=dim, tiled=True)  19.5 us
  transfers between devices with their start and end apart: 21, of which 17 were waited for; matrix products, arithmetic and copies ran while one was open for 32% of the time, Pallas kernels for 0%

profile of v1, /device:TPU:3, one launch (start us, length us, event | category | flops | bytes accessed | tf_op | source)
XLA Modules:
  0.0 433.0 jit_solution(17305853850601862335)
XLA Ops:
  10.4 1.9 collective-permute-start
  12.3 1.0 collective-permute-done
  13.3 2.3 collective-permute-start.2
  16.6 2.3 collective-permute-start.4
  20.9 1.4 collective-permute-start.6
  22.6 2.2 collective-permute-start.7
  25.9 3.4 collective-permute-start.9
  30.2 3.7 collective-permute-start.11
  34.7 3.7 collective-permute-start.13
  40.9 7.4 %dynamic_update_slice.48 = bf16[2,64,2048]{1,2,0:T(8,128)(2,1)S(1)} dynamic-update-slice(bf16[2,64,2048]{1,2,0:T(8,128)(2,1)S(1)} %broadcast_in_dim.5, bf16[2,4,2048]{1,2,0:T(8,128)(2,1)S(1)} %copy.51, s32[]{:T(128)} %constant.99.clone.1, s32[]{:T(128)S(6)} %select_n.111, s32[]{:T(128)} %constant.99.clone.1) | dynamic-update-slice | bytes 65540 | tf_op jit(solution)/shard_map/dynamic_update_slice | solution.py:118
  48.8 4.1 dynamic_update_slice.49
  53.4 7.4 %dynamic_update_slice.50 = bf16[2,64,2048]{1,2,0:T(8,128)(2,1)S(1)} dynamic-update-slice(bf16[2,64,2048]{1,2,0:T(8,128)(2,1)S(1)} %dynamic_update_slice.49, bf16[2,4,2048]{1,2,0:T(8,128)(2,1)S(1)} %copy.53, s32[]{:T(128)} %constant.99.clone.1, s32[]{:T(128)S(6)} %select_n.115, s32[]{:T(128)} %constant.99.clone.1) | dynamic-update-slice | bytes 65540 | tf_op jit(solution)/shard_map/dynamic_update_slice | solution.py:128
  61.4 7.4 %dynamic_update_slice.51 = bf16[2,64,2048]{1,2,0:T(8,128)(2,1)S(1)} dynamic-update-slice(bf16[2,64,2048]{1,2,0:T(8,128)(2,1)S(1)} %dynamic_update_slice.50, bf16[2,4,2048]{1,2,0:T(8,128)(2,1)S(1)} %copy.54, s32[]{:T(128)} %constant.99.clone.1, s32[]{:T(128)S(6)} %select_n.117, s32[]{:T(128)} %constant.99.clone.1) | dynamic-update-slice | bytes 65540 | tf_op jit(solution)/shard_map/dynamic_update_slice | solution.py:123
  69.3 7.4 %dynamic_update_slice.52 = bf16[2,64,2048]{1,2,0:T(8,128)(2,1)S(1)} dynamic-update-slice(bf16[2,64,2048]{1,2,0:T(8,128)(2,1)S(1)} %dynamic_update_slice.51, bf16[2,4,2048]{1,2,0:T(8,128)(2,1)S(1)} %copy.55, s32[]{:T(128)} %constant.99.clone.1, s32[]{:T(128)S(6)} %select_n.119, s32[]{:T(128)} %constant.99.clone.1) | dynamic-update-slice | bytes 65540 | tf_op jit(solution)/shard_map/dynamic_update_slice | solution.py:128
  77.2 7.4 %dynamic_update_slice.53 = bf16[2,64,2048]{1,2,0:T(8,128)(2,1)S(1)} dynamic-update-slice(bf16[2,64,2048]{1,2,0:T(8,128)(2,1)S(1)} %dynamic_update_slice.52, bf16[2,4,2048]{1,2,0:T(8,128)(2,1)S(1)} %copy.56, s32[]{:T(128)} %constant.99.clone.1, s32[]{:T(128)S(6)} %select_n.121, s32[]{:T(128)} %constant.99.clone.1) | dynamic-update-slice | bytes 65540 | tf_op jit(solution)/shard_map/dynamic_update_slice | solution.py:123
  85.1 7.4 %dynamic_update_slice.54 = bf16[2,64,2048]{1,2,0:T(8,128)(2,1)S(1)} dynamic-update-slice(bf16[2,64,2048]{1,2,0:T(8,128)(2,1)S(1)} %dynamic_update_slice.53, bf16[2,4,2048]{1,2,0:T(8,128)(2,1)S(1)} %copy.57, s32[]{:T(128)} %constant.99.clone.1, s32[]{:T(128)S(6)} %select_n.123, s32[]{:T(128)} %constant.99.clone.1) | dynamic-update-slice | bytes 65540 | tf_op jit(solution)/shard_map/dynamic_update_slice | solution.py:128
  93.1 7.4 %dynamic_update_slice.55 = bf16[2,64,2048]{1,2,0:T(8,128)(2,1)S(1)} dynamic-update-slice(bf16[2,64,2048]{1,2,0:T(8,128)(2,1)S(1)} %dynamic_update_slice.54, bf16[2,4,2048]{1,2,0:T(8,128)(2,1)S(1)} %copy.58, s32[]{:T(128)} %constant.99.clone.1, s32[]{:T(128)S(6)} %select_n.125, s32[]{:T(128)} %constant.99.clone.1) | dynamic-update-slice | bytes 65540 | tf_op jit(solution)/shard_map/dynamic_update_slice | solution.py:123
  101.0 7.4 %dynamic_update_slice.56 = bf16[2,64,2048]{1,2,0:T(8,128)(2,1)S(1)} dynamic-update-slice(bf16[2,64,2048]{1,2,0:T(8,128)(2,1)S(1)} %dynamic_update_slice.55, bf16[2,4,2048]{1,2,0:T(8,128)(2,1)S(1)} %copy.59, s32[]{:T(128)} %constant.99.clone.1, s32[]{:T(128)S(6)} %select_n.127, s32[]{:T(128)} %constant.99.clone.1) | dynamic-update-slice | bytes 65540 | tf_op jit(solution)/shard_map/dynamic_update_slice | solution.py:128
  108.9 7.4 %dynamic_update_slice.57 = bf16[2,64,2048]{1,2,0:T(8,128)(2,1)S(1)} dynamic-update-slice(bf16[2,64,2048]{1,2,0:T(8,128)(2,1)S(1)} %dynamic_update_slice.56, bf16[2,4,2048]{1,2,0:T(8,128)(2,1)S(1)} %copy.60, s32[]{:T(128)} %constant.99.clone.1, s32[]{:T(128)S(6)} %select_n.129, s32[]{:T(128)} %constant.99.clone.1) | dynamic-update-slice | bytes 65540 | tf_op jit(solution)/shard_map/dynamic_update_slice | solution.py:123
  116.9 7.6 %dynamic_update_slice.58 = bf16[2,64,2048]{1,2,0:T(8,128)(2,1)S(1)} dynamic-update-slice(bf16[2,64,2048]{1,2,0:T(8,128)(2,1)S(1)} %dynamic_update_slice.57, bf16[2,4,2048]{1,2,0:T(8,128)(2,1)S(1)} %copy.61, s32[]{:T(128)} %constant.99.clone.1, s32[]{:T(128)S(6)} %select_n.131, s32[]{:T(128)} %constant.99.clone.1) | dynamic-update-slice | bytes 65540 | tf_op jit(solution)/shard_map/dynamic_update_slice | solution.py:128
  125.0 7.4 %dynamic_update_slice.59 = bf16[2,64,2048]{1,2,0:T(8,128)(2,1)S(1)} dynamic-update-slice(bf16[2,64,2048]{1,2,0:T(8,128)(2,1)S(1)} %dynamic_update_slice.58, bf16[2,4,2048]{1,2,0:T(8,128)(2,1)S(1)} %copy.62, s32[]{:T(128)} %constant.99.clone.1, s32[]{:T(128)S(6)} %select_n.133, s32[]{:T(128)} %constant.99.clone.1) | dynamic-update-slice | bytes 65540 | tf_op jit(solution)/shard_map/dynamic_update_slice | solution.py:123
  132.9 7.4 %dynamic_update_slice.60 = bf16[2,64,2048]{1,2,0:T(8,128)(2,1)S(1)} dynamic-update-slice(bf16[2,64,2048]{1,2,0:T(8,128)(2,1)S(1)} %dynamic_update_slice.59, bf16[2,4,2048]{1,2,0:T(8,128)(2,1)S(1)} %copy.63, s32[]{:T(128)} %constant.99.clone.1, s32[]{:T(128)S(6)} %select_n.135, s32[]{:T(128)} %constant.99.clone.1) | dynamic-update-slice | bytes 65540 | tf_op jit(solution)/shard_map/dynamic_update_slice | solution.py:128
  140.9 7.4 %dynamic_update_slice.61 = bf16[2,64,2048]{1,2,0:T(8,128)(2,1)S(1)} dynamic-update-slice(bf16[2,64,2048]{1,2,0:T(8,128)(2,1)S(1)} %dynamic_update_slice.60, bf16[2,4,2048]{1,2,0:T(8,128)(2,1)S(1)} %copy.64, s32[]{:T(128)} %constant.99.clone.1, s32[]{:T(128)S(6)} %select_n.137, s32[]{:T(128)} %constant.99.clone.1) | dynamic-update-slice | bytes 65540 | tf_op jit(solution)/shard_map/dynamic_update_slice | solution.py:123
  148.3 1.3 copy.65
  149.6 7.4 %dynamic_update_slice.62 = bf16[2,64,2048]{1,2,0:T(8,128)(2,1)S(1)} dynamic-update-slice(bf16[2,64,2048]{1,2,0:T(8,128)(2,1)S(1)} %dynamic_update_slice.61, bf16[2,4,2048]{1,2,0:T(8,128)(2,1)S(1)} %copy.65, s32[]{:T(128)} %constant.99.clone.1, s32[]{:T(128)S(6)} %select_n.139, s32[]{:T(128)} %constant.99.clone.1) | dynamic-update-slice | bytes 65540 | tf_op jit(solution)/shard_map/dynamic_update_slice | solution.py:128
  157.0 2.2 copy.66
  159.2 11.4 %dynamic_update_slice.63 = bf16[2,64,2048]{1,2,0:T(8,128)(2,1)S(1)} dynamic-update-slice(bf16[2,64,2048]{1,2,0:T(8,128)(2,1)S(1)} %dynamic_update_slice.62, bf16[2,4,2048]{1,2,0:T(8,128)(2,1)} %copy.66, s32[]{:T(128)} %constant.99.clone.1, s32[]{:T(128)S(6)} %select_n.141, s32[]{:T(128)} %constant.99.clone.1) | dynamic-update-slice | bytes 65540 | tf_op jit(solution)/shard_map/dynamic_update_slice | solution.py:123
  170.6 2.2 multiply_reduce_fusion
  174.2 40.6 %all_to_all.20 = bf16[16,16,2048]{2,1,0:T(8,128)(2,1)S(1)} all-to-all(bf16[16,16,2048]{2,1,0:T(8,128)(2,1)S(1)} %broadcast_in_dim.4), channel_id=1, replica_groups=mesh['sp_0'=8,'sp_1'=4,'tp'=16] {'tp'}, dimensions={0} | all-to-all | bytes 2097152 | tf_op jit(solution)/shard_map/all_to_all | solution.py:16
  214.8 1.7 convolution_convert_fusion.5
  216.4 46.2 %all-gather.2.cloned.1.call-done = bf16[2048,1,514]{2,0,1:T(8,128)(2,1)} async-done(((bf16[64,1,514]{2,0,1:T(8,128)(2,1)}), bf16[2048,1,514]{2,0,1:T(8,128)(2,1)}) %all-gather.2.cloned.1.call-update) | async-done | bytes 2105360 | tf_op jit(solution)/shard_map/all_gather | solution.py:35
  262.6 1.9 convert_reduce_fusion.1
  264.5 3.1 fusion.3
  267.6 3.3 fusion.5
  270.9 1.5 fusion.6
  272.4 4.0 fusion.8
  276.3 5.0 %fusion.4 = bf16[256,2048]{1,0:T(8,128)(2,1)} fusion(f32[256,2048]{1,0:T(8,128)} %fusion.8, bf16[2048,256]{1,0:T(8,128)(2,1)S(1)} %copy-done, f32[2048,256]{1,0:T(8,128)} %fusion.3, bf16[2048,1,514]{2,0,1:T(8,128)(2,1)} %all-gather.2.cloned.1.call-done), kind=kOutput, calls=%fused_computation.7 | convolution fusion | flops 538509312 | bytes 7340032 | tf_op jit(solution)/shard_map/dot_general | solution.py:65
  281.3 11.8 %all-to-all-start.2 = ((bf16[16,16,2048]{2,1,0:T(8,128)(2,1)}), bf16[16,16,2048]{2,1,0:T(8,128)(2,1)}, u32[]{:S(2)}, u32[]{:S(2)}) async-start(bf16[16,16,2048]{2,1,0:T(8,128)(2,1)} %bitcast.20), calls=%async_computation.3 | async-start | bytes 2097152 | tf_op jit(solution)/shard_map/all_to_all | solution.py:54
  293.1 19.5 %reduce-scatter.5.cloned.1.call-done = bf16[256,1,256]{0,2,1:T(8,128)(2,1)} async-done(((bf16[2048,1,256]{0,2,1:T(8,128)(2,1)}), bf16[256,1,256]{0,2,1:T(8,128)(2,1)}) %reduce-scatter.5.cloned.1.call-update) | async-done | bytes 131088 | tf_op jit(solution)/shard_map/reduce_scatter | solution.py:43
  312.6 1.7 copy.74
  314.3 26.3 %reduce-scatter.7.cloned.1.call-done = bf16[64,256]{1,0:T(8,128)(2,1)} async-done(((bf16[256,256]{1,0:T(8,128)(2,1)}), bf16[64,256]{1,0:T(8,128)(2,1)}) %reduce-scatter.7.cloned.1.call-update) | async-done | bytes 32784 | tf_op jit(solution)/shard_map/reshape | solution.py:177
  340.6 1.3 convolution_convert_fusion.1
  342.7 9.5 %all-to-all-start.1 = ((bf16[16,4,2048]{2,1,0:T(4,128)(2,1)}), bf16[16,4,2048]{2,1,0:T(4,128)(2,1)S(1)}, u32[]{:S(2)}, u32[]{:S(2)}) async-start(bf16[16,4,2048]{2,1,0:T(4,128)(2,1)} %reshape.145), calls=%async_computation.2 | async-start | bytes 524288 | tf_op jit(solution)/shard_map/all_to_all | solution.py:54
  352.2 1.7 fusion.20
  353.9 9.8 %all-to-all-done.1 = bf16[16,4,2048]{2,1,0:T(4,128)(2,1)S(1)} async-done(((bf16[16,4,2048]{2,1,0:T(4,128)(2,1)}), bf16[16,4,2048]{2,1,0:T(4,128)(2,1)S(1)}, u32[]{:S(2)}, u32[]{:S(2)}) %all-to-all-start.1) | async-done | bytes 262176 | tf_op jit(solution)/shard_map/all_to_all | solution.py:54
  363.7 10.3 %all-to-all-start.3 = ((f32[32,64,256]{2,1,0:T(8,128)}), f32[32,64,256]{2,1,0:T(8,128)S(1)}, u32[]{:S(2)}, u32[]{:S(2)}) async-start(f32[32,64,256]{2,1,0:T(8,128)} %fusion.20), calls=%async_computation.4 | async-start | bytes 4194304 | tf_op jit(solution)/shard_map/all_to_all | solution.py:60
  374.0 2.0 convert_reduce_fusion
  377.0 48.7 %all-to-all-done.3 = f32[32,64,256]{2,1,0:T(8,128)S(1)} async-done(((f32[32,64,256]{2,1,0:T(8,128)}), f32[32,64,256]{2,1,0:T(8,128)S(1)}, u32[]{:S(2)}, u32[]{:S(2)}) %all-to-all-start.3) | async-done | bytes 2097184 | tf_op jit(solution)/shard_map/all_to_all | solution.py:60
  (88 shorter events, 22.2 us)
Async XLA Ops:
  7.2 260.4 %copy-start = (bf16[2048,256]{1,0:T(8,128)(2,1)S(1)}, bf16[2048,256]{1,0:T(8,128)(2,1)}, u32[]{:S(2)}) copy-start(bf16[2048,256]{1,0:T(8,128)(2,1)} %param.15) | copy-start | bytes 3145732
  7.2 255.4 %all-gather.2.cloned.1.call-start = ((), (), s32[]{:S(2)}) async-start(), calls=%async_computation.6 | async-start | bytes 2703360 | tf_op jit(solution)/shard_map/all_gather | solution.py:35
  10.4 2.9 collective-permute-start
  12.3 3.3 collective-permute-start.1
  13.3 3.3 collective-permute-start.2
  15.6 3.6 collective-permute-start.3
  16.6 4.3 collective-permute-start.4
  19.3 3.3 collective-permute-start.5
  20.9 4.6 %collective-permute-start.6 = (bf16[2,4,2048]{2,1,0:T(4,128)(2,1)S(1)}, bf16[2,4,2048]{2,1,0:T(4,128)(2,1)S(1)}, u32[]{:S(2)}, u32[]{:S(2)}) collective-permute-start(bf16[2,4,2048]{2,1,0:T(4,128)(2,1)S(1)} %collective-permute-done.4), channel_id=1, source_target_pairs={{0,1},{1,2},{2,3},{3,4},{4,5},{5,6},{6,7},{7,8},{8,9},{9,10},{10,1... | collective-permute-start | bytes 98312 | tf_op jit(solution)/shard_map/ppermute | solution.py:122
  22.6 3.3 collective-permute-start.7
  25.4 4.6 %collective-permute-start.8 = (bf16[2,4,2048]{2,1,0:T(4,128)(2,1)S(1)}, bf16[2,4,2048]{2,1,0:T(4,128)(2,1)S(1)}, u32[]{:S(2)}, u32[]{:S(2)}) collective-permute-start(bf16[2,4,2048]{2,1,0:T(4,128)(2,1)S(1)} %collective-permute-done.6), channel_id=1, source_target_pairs={{0,1},{1,2},{2,3},{3,4},{4,5},{5,6},{6,7},{7,8},{8,9},{9,10},{10,1... | collective-permute-start | bytes 98312 | tf_op jit(solution)/shard_map/ppermute | solution.py:122
  25.9 4.2 collective-permute-start.9
  30.0 4.6 %collective-permute-start.10 = (bf16[2,4,2048]{2,1,0:T(4,128)(2,1)S(1)}, bf16[2,4,2048]{2,1,0:T(4,128)(2,1)S(1)}, u32[]{:S(2)}, u32[]{:S(2)}) collective-permute-start(bf16[2,4,2048]{2,1,0:T(4,128)(2,1)S(1)} %collective-permute-done.8), channel_id=1, source_target_pairs={{0,1},{1,2},{2,3},{3,4},{4,5},{5,6},{6,7},{7,8},{8,9},{9,10},{10,1... | collective-permute-start | bytes 98312 | tf_op jit(solution)/shard_map/ppermute | solution.py:122
  30.2 10.6 %copy-start.10 = (bf16[2,4,2048]{2,1,0:T(4,128)(2,1)}, bf16[2,4,2048]{2,1,0:T(4,128)(2,1)S(1)}, u32[]{:S(2)}) copy-start(bf16[2,4,2048]{2,1,0:T(4,128)(2,1)S(1)} %collective-permute-done.9) | copy-start | bytes 98308
  30.2 4.6 %collective-permute-start.11 = (bf16[2,4,2048]{2,1,0:T(4,128)(2,1)S(1)}, bf16[2,4,2048]{2,1,0:T(4,128)(2,1)S(1)}, u32[]{:S(2)}, u32[]{:S(2)}) collective-permute-start(bf16[2,4,2048]{2,1,0:T(4,128)(2,1)S(1)} %collective-permute-done.9), channel_id=1, source_target_pairs={{0,15},{1,0},{2,1},{3,2},{4,3},{5,4},{6,5},{7,6},{8,7},{9,8},{10,9... | collective-permute-start | bytes 98312 | tf_op jit(solution)/shard_map/ppermute | solution.py:127
  34.5 6.2 %copy-start.12 = (bf16[2,4,2048]{2,1,0:T(4,128)(2,1)}, bf16[2,4,2048]{2,1,0:T(4,128)(2,1)S(1)}, u32[]{:S(2)}) copy-start(bf16[2,4,2048]{2,1,0:T(4,128)(2,1)S(1)} %collective-permute-done.10) | copy-start | bytes 98308
  34.6 4.6 %collective-permute-start.12 = (bf16[2,4,2048]{2,1,0:T(4,128)(2,1)S(1)}, bf16[2,4,2048]{2,1,0:T(4,128)(2,1)S(1)}, u32[]{:S(2)}, u32[]{:S(2)}) collective-permute-start(bf16[2,4,2048]{2,1,0:T(4,128)(2,1)S(1)} %collective-permute-done.10), channel_id=1, source_target_pairs={{0,1},{1,2},{2,3},{3,4},{4,5},{5,6},{6,7},{7,8},{8,9},{9,10},{10,1... | collective-permute-start | bytes 98312 | tf_op jit(solution)/shard_map/ppermute | solution.py:122
  34.7 113.6 %collective-permute-start.13 = (bf16[2,4,2048]{2,1,0:T(4,128)(2,1)S(1)}, bf16[2,4,2048]{2,1,0:T(4,128)(2,1)}, u32[]{:S(2)}, u32[]{:S(2)}) collective-permute-start(bf16[2,4,2048]{2,1,0:T(4,128)(2,1)S(1)} %collective-permute-done.11), channel_id=1, source_target_pairs={{0,15},{1,0},{2,1},{3,2},{4,3},{5,4},{6,5},{7,6},{8,7},{9,8},{10,9... | collective-permute-start | bytes 98312 | tf_op jit(solution)/shard_map/ppermute | solution.py:127
  39.1 117.9 %collective-permute-start.14 = (bf16[2,4,2048]{2,1,0:T(4,128)(2,1)S(1)}, bf16[2,4,2048]{2,1,0:T(4,128)(2,1)}, u32[]{:S(2)}, u32[]{:S(2)}) collective-permute-start(bf16[2,4,2048]{2,1,0:T(4,128)(2,1)S(1)} %collective-permute-done.12), channel_id=1, source_target_pairs={{0,1},{1,2},{2,3},{3,4},{4,5},{5,6},{6,7},{7,8},{8,9},{9,10},{10,1... | collective-permute-start | bytes 98312 | tf_op jit(solution)/shard_map/ppermute | solution.py:122
  108.4 7.9 %copy-start.11 = (bf16[2,4,2048]{2,1,0:T(4,128)(2,1)S(1)}, bf16[2,4,2048]{2,1,0:T(4,128)(2,1)}, u32[]{:S(2)}) copy-start(bf16[2,4,2048]{2,1,0:T(4,128)(2,1)} %copy-done.10) | copy-start | bytes 98308
  116.4 8.1 %copy-start.13 = (bf16[2,4,2048]{2,1,0:T(4,128)(2,1)S(1)}, bf16[2,4,2048]{2,1,0:T(4,128)(2,1)}, u32[]{:S(2)}) copy-start(bf16[2,4,2048]{2,1,0:T(4,128)(2,1)} %copy-done.12) | copy-start | bytes 98308
  157.0 13.6 %copy-start.9 = (bf16[64,256]{1,0:T(8,128)(2,1)S(1)}, bf16[64,256]{1,0:T(8,128)(2,1)}, u32[]{:S(2)}) copy-start(bf16[64,256]{1,0:T(8,128)(2,1)} %param.17) | copy-start | bytes 98308
  159.2 13.7 %copy-start.4 = (bf16[2048,256]{1,0:T(8,128)(2,1)S(1)}, bf16[2048,256]{1,0:T(8,128)(2,1)}, u32[]{:S(2)}) copy-start(bf16[2048,256]{1,0:T(8,128)(2,1)} %param.13) | copy-start | bytes 3145732
  170.6 3.6 copy-start.1
  170.6 3.5 copy-start.8
  174.0 138.7 %reduce-scatter.5.cloned.1.call-start = ((), (), s32[]{:S(2)}) async-start(), calls=%async_computation.7 | async-start | bytes 1179648 | tf_op jit(solution)/shard_map/reduce_scatter | solution.py:43
  270.9 1.5 copy-start.3
  281.3 59.3 %copy-start.5 = (bf16[2048,256]{1,0:T(8,128)(2,1)S(1)}, bf16[2048,256]{1,0:T(8,128)(2,1)}, u32[]{:S(2)}) copy-start(bf16[2048,256]{1,0:T(8,128)(2,1)} %param.13) | copy-start | bytes 3145732
  281.3 70.8 %copy-start.2 = (bf16[2,64,2048]{1,2,0:T(8,128)(2,1)S(1)}, bf16[2,64,2048]{1,2,0:T(8,128)(2,1)}, u32[]{:S(2)}) copy-start(bf16[2,64,2048]{1,2,0:T(8,128)(2,1)} %copy-done.1) | copy-start | bytes 1572868
  281.3 61.3 %all-to-all-start.2 = ((bf16[16,16,2048]{2,1,0:T(8,128)(2,1)}), bf16[16,16,2048]{2,1,0:T(8,128)(2,1)}, u32[]{:S(2)}, u32[]{:S(2)}) async-start(bf16[16,16,2048]{2,1,0:T(8,128)(2,1)} %bitcast.20), calls=%async_computation.3 | async-start | bytes 2097152 | tf_op jit(solution)/shard_map/all_to_all | solution.py:54
  293.1 47.5 %reduce-scatter.7.cloned.1.call-start = ((), (), s32[]{:S(2)}) async-start(), calls=%async_computation.8 | async-start | bytes 163840 | tf_op jit(solution)/shard_map/reshape | solution.py:177
  340.6 11.6 %copy-start.7 = (bf16[64,256]{1,0:T(8,128)(2,1)S(1)}, bf16[64,256]{1,0:T(8,128)(2,1)}, u32[]{:S(2)}) copy-start(bf16[64,256]{1,0:T(8,128)(2,1)} %reduce-scatter.7.cloned.1.call-done) | copy-start | bytes 98308
  342.7 21.1 %all-to-all-start.1 = ((bf16[16,4,2048]{2,1,0:T(4,128)(2,1)}), bf16[16,4,2048]{2,1,0:T(4,128)(2,1)S(1)}, u32[]{:S(2)}, u32[]{:S(2)}) async-start(bf16[16,4,2048]{2,1,0:T(4,128)(2,1)} %reshape.145), calls=%async_computation.2 | async-start | bytes 524288 | tf_op jit(solution)/shard_map/all_to_all | solution.py:54
  353.9 22.2 %copy-start.6 = (bf16[4,2048]{1,0:T(4,128)(2,1)S(1)}, bf16[4,2048]{1,0:T(4,128)(2,1)}, u32[]{:S(2)}) copy-start(bf16[4,2048]{1,0:T(4,128)(2,1)} %param.10) | copy-start | bytes 49156
  363.7 62.0 %all-to-all-start.3 = ((f32[32,64,256]{2,1,0:T(8,128)}), f32[32,64,256]{2,1,0:T(8,128)S(1)}, u32[]{:S(2)}, u32[]{:S(2)}) async-start(f32[32,64,256]{2,1,0:T(8,128)} %fusion.20), calls=%async_computation.4 | async-start | bytes 4194304 | tf_op jit(solution)/shard_map/all_to_all | solution.py:60
Sparse Core Ops, SparseCore 0:
  174.1 88.4 all-gather.1
  272.5 40.1 reduce-scatter.4
  316.0 24.5 reduce-scatter.6
